TPU v7x, 32 devices: a whole 2x2x4 slice. The times are simulated.
32 devices in a mesh: rep: 2 (over y), fs: 4 (over z), tp: 4 (over x, core).
Axes of the slice: x: 2, y: 2, z: 4, core: 2. Of those that a mesh axis runs over, the one named last changes fastest.
Arguments:
- tokens: bfloat16 [4096, 2048], P(('rep', 'fs', 'tp')), may hold values from -6 to 6
- norm_gain: float32 [2048], replicated, may hold values from 0.1 to 1.9
- w_gate: bfloat16 [2048, 3072], P('fs', 'tp'), may hold values from -0.125 to 0.125
- w_up: bfloat16 [2048, 3072], P('fs', 'tp'), may hold values from -0.125 to 0.125
- w_down: bfloat16 [3072, 2048], P('tp', 'fs'), may hold values from -0.109375 to 0.109375
- post_gain: float32 [2048], replicated, may hold values from 0.1 to 1.9
Outputs:
- result: bfloat16 [4096, 2048], P(('rep', 'fs', 'tp'))
All inputs are finite; a program needn't handle non-finite values.
Results may differ from a plain program's by a relative error of at most 0.014.
Values may be sent and summed in bfloat16 or wider, within the bound.
A program may use at most 64 MiB of HBM per device.

v0:
```python
import jax
import jax.numpy as jnp
from jax import lax
from jax.sharding import PartitionSpec as P

EPS = 1e-06


def rms_scale(values, gain):
    return values * lax.rsqrt(jnp.mean(values * values, axis=-1, keepdims=True) + EPS) * gain


def body(tokens, norm_gain, w_gate, w_up, w_down, post_gain):
    own_normed = rms_scale(tokens.astype(jnp.float32), norm_gain).astype(jnp.bfloat16)
    normed = lax.all_gather(own_normed, "tp", axis=0, tiled=True)
    gate = jnp.dot(
        normed, lax.all_gather(w_gate, "fs", axis=0, tiled=True), preferred_element_type=jnp.float32
    )
    up = jnp.dot(
        normed, lax.all_gather(w_up, "fs", axis=0, tiled=True), preferred_element_type=jnp.float32
    )
    hidden = (jax.nn.silu(gate) * up).astype(jnp.bfloat16)
    terms = jnp.dot(
        hidden, lax.all_gather(w_down, "fs", axis=1, tiled=True), preferred_element_type=jnp.float32
    )
    summed = lax.psum_scatter(
        terms.astype(jnp.bfloat16), "tp", scatter_dimension=0, tiled=True
    ).astype(jnp.float32)
    return rms_scale(summed, post_gain).astype(jnp.bfloat16)


def solution(mesh):
    return jax.shard_map(
        body,
        mesh=mesh,
        in_specs=(
            P(("rep", "fs", "tp"), None),
            P(),
            P("fs", "tp"),
            P("fs", "tp"),
            P("tp", "fs"),
            P(),
        ),
        out_specs=P(("rep", "fs", "tp"), None),
        check_vma=False,
    )
```

profile of v0, /device:TPU:0, one launch (start us, length us, event | category | flops | bytes accessed | tf_op | source)
XLA Modules:
  0.0 276.0 jit_solution(9713884520916390494)
XLA Ops:
  6.5 0.0 all-gather.5.cloned.1.call-start
  6.5 1.2 fusion
  7.8 2.0 fusion.2
  9.8 0.0 all-gather.5.cloned.1.call-update
  9.8 0.0 all-gather.7.cloned.1.call-start
  9.9 0.7 all-gather.7.cloned.1.call-update
  10.6 0.0 all-gather.11.cloned.1.call-start
  10.6 0.7 all-gather.11.cloned.1.call-update
  11.3 0.0 all-gather.9.cloned.1.call-start
  11.4 0.5 all-gather.9.cloned.1.call-update
  11.9 0.0 reduce-scatter.2.cloned.1.call-start
  11.9 23.3 %all-gather.5.cloned.1.call-done = bf16[512,2048]{1,0:T(8,128)(2,1)} async-done(((bf16[128,2048]{1,0:T(8,128)(2,1)}), bf16[512,2048]{1,0:T(8,128)(2,1)}) %all-gather.5.cloned.1.call-update) | async-done | bytes 2097168 | tf_op jit(solution)/shard_map/all_gather | solution.py:15
  35.3 0.0 copy-start.1
  35.3 65.0 %all-gather.7.cloned.1.call-done = bf16[2048,768]{1,0:T(8,128)(2,1)} async-done(((bf16[512,768]{1,0:T(8,128)(2,1)}), bf16[2048,768]{1,0:T(8,128)(2,1)}) %all-gather.7.cloned.1.call-update) | async-done | bytes 3145744 | tf_op jit(solution)/shard_map/all_gather | solution.py:17
  100.3 5.5 %fusion.7 = f32[512,768]{1,0:T(8,128)} fusion(bf16[512,2048]{1,0:T(8,128)(2,1)} %all-gather.5.cloned.1.call-done, bf16[2048,768]{1,0:T(8,128)(2,1)} %all-gather.7.cloned.1.call-done), kind=kOutput, calls=%fused_computation.15 | convolution fusion | flops 1610612736 | bytes 6815744 | tf_op jit(solution)/shard_map/dot_general | solution.py:16
  105.8 58.2 %all-gather.11.cloned.1.call-done = bf16[768,2048]{1,0:T(8,128)(2,1)} async-done(((bf16[768,512]{1,0:T(8,128)(2,1)}), bf16[768,2048]{1,0:T(8,128)(2,1)}) %all-gather.11.cloned.1.call-update) | async-done | bytes 3145744 | tf_op jit(solution)/shard_map/all_gather | solution.py:24
  164.0 63.5 %all-gather.9.cloned.1.call-done = bf16[2048,768]{1,0:T(8,128)(2,1)} async-done(((bf16[512,768]{1,0:T(8,128)(2,1)}), bf16[2048,768]{1,0:T(8,128)(2,1)}) %all-gather.9.cloned.1.call-update) | async-done | bytes 3145744 | tf_op jit(solution)/shard_map/all_gather | solution.py:20
  227.5 0.0 copy-done.1
  227.6 8.6 %convolution_convert_fusion = bf16[512,2048]{1,0:T(8,128)(2,1)} fusion(bf16[768,2048]{1,0:T(8,128)(2,1)} %all-gather.11.cloned.1.call-done, f32[512,768]{1,0:T(8,128)} %fusion.7, bf16[512,2048]{1,0:T(8,128)(2,1)S(1)} %copy-done.1, bf16[2048,768]{1,0:T(8,128)(2,1)} %all-gather.9.cloned.1.call-done), kind=kOutput, calls=%fused_computation | convolution fusion | flops 3224633344 | bytes 12058624 | tf_op jit(solution)/shard_map/dot_general | solution.py:23
  236.2 0.0 copy-start
  236.2 0.0 reduce-scatter.2.cloned.1.call-update
  236.2 30.0 %reduce-scatter.2.cloned.1.call-done = bf16[128,2048]{1,0:T(8,128)(2,1)} async-done(((bf16[512,2048]{1,0:T(8,128)(2,1)}), bf16[128,2048]{1,0:T(8,128)(2,1)}) %reduce-scatter.2.cloned.1.call-update) | async-done | bytes 524304 | tf_op jit(solution)/shard_map/reduce_scatter | solution.py:26
  266.2 1.2 fusion.3
  267.4 0.0 copy-done
  267.4 2.0 fusion.5
  (2 shorter events, 0.0 us)
Async XLA Ops:
  6.5 28.7 %all-gather.5.cloned.1.call-start = ((), (), s32[]{:S(2)}) async-start(), calls=%async_computation.1 | async-start | bytes 2621440 | tf_op jit(solution)/shard_map/all_gather | solution.py:15
  9.8 90.5 %all-gather.7.cloned.1.call-start = ((), (), s32[]{:S(2)}) async-start(), calls=%async_computation.2 | async-start | bytes 3932160 | tf_op jit(solution)/shard_map/all_gather | solution.py:17
  10.6 153.4 %all-gather.11.cloned.1.call-start = ((), (), s32[]{:S(2)}) async-start(), calls=%async_computation.4 | async-start | bytes 3932160 | tf_op jit(solution)/shard_map/all_gather | solution.py:24
  11.3 216.2 %all-gather.9.cloned.1.call-start = ((), (), s32[]{:S(2)}) async-start(), calls=%async_computation.3 | async-start | bytes 3932160 | tf_op jit(solution)/shard_map/all_gather | solution.py:20
  11.9 254.3 %reduce-scatter.2.cloned.1.call-start = ((), (), s32[]{:S(2)}) async-start(), calls=%async_computation.5 | async-start | bytes 2621440 | tf_op jit(solution)/shard_map/reduce_scatter | solution.py:26
  35.3 192.3 %copy-start.1 = (bf16[512,2048]{1,0:T(8,128)(2,1)S(1)}, bf16[512,2048]{1,0:T(8,128)(2,1)}, u32[]{:S(2)}) copy-start(bf16[512,2048]{1,0:T(8,128)(2,1)} %all-gather.5.cloned.1.call-done) | copy-start | bytes 6291460
  236.2 31.2 %copy-start = (f32[2048]{0:T(1024)S(1)}, f32[2048]{0:T(1024)}, u32[]{:S(2)}) copy-start(f32[2048]{0:T(1024)} %param.11) | copy-start | bytes 24580
Sparse Core Ops, SparseCore 0:
  9.9 25.2 all-gather.4
  36.8 63.4 all-gather.6
  101.9 62.0 all-gather.10
  165.4 62.0 all-gather.8
  236.3 29.7 reduce-scatter.1
where the time goes:
time: 276 us
  waiting for transfers between devices  242 us (88%)
  matrix products  14.1 us (5%)
  between operations  13.1 us (5%)
  other arithmetic  6.53 us (2%)
    all_gather x1, waiting for transfers between devices, body(): lax.all_gather(w_gate, 'fs', axis=0, tiled=True)  65 us
    all_gather x1, waiting for transfers between devices, body(): lax.all_gather(w_up, 'fs', axis=0, tiled=True)  63.5 us
    all_gather x1, waiting for transfers between devices, body(): lax.all_gather(w_down, 'fs', axis=1, tiled=True)  58.2 us
    reduce_scatter x1, waiting for transfers between devices, body(): lax.psum_scatter(terms.astype(jnp.bfloat16), 'tp', scatter_dimension=0, t...  30 us
    all_gather x1, waiting for transfers between devices, body(): normed = lax.all_gather(own_normed, 'tp', axis=0, tiled=True)  23.3 us
    dot_general x1, matrix products, body(): jnp.dot(hidden, lax.all_gather(w_down, 'fs', axis=1, tiled=True), preferr...  8.63 us
  transfers between devices with their start and end apart: 5, of which 5 were waited for; matrix products, arithmetic and copies ran while one was open for 2% of the time, Pallas kernels for 0%

commit v1 on v0

--- a/solution.py
+++ b/solution.py
@@ -1,3 +1,4 @@
+import functools
 import jax
 import jax.numpy as jnp
 from jax import lax
@@ -6,13 +7,28 @@
 EPS = 1e-06
 
 
+def _place_rows(xx, along_axis):
+    total_devices = lax.axis_size(along_axis)
+    series = list(map(lambda dev_j: (dev_j, (dev_j + 1) % total_devices), range(total_devices)))
+    then = [None] * total_devices
+    then[total_devices - 1] = xx
+    for s in range(total_devices - 2, -1, -1):
+        then[s] = lax.ppermute(then[s + 1], along_axis, series)
+    oldest = jnp.concatenate(then, 0)
+    y2 = (lax.axis_index(along_axis) + 1) * xx.shape[0]
+    return jnp.roll(oldest, y2, axis=0)
+
+
+rest_pools = functools.partial(_place_rows, along_axis="tp")
+
+
 def rms_scale(values, gain):
     return values * lax.rsqrt(jnp.mean(values * values, axis=-1, keepdims=True) + EPS) * gain
 
 
 def body(tokens, norm_gain, w_gate, w_up, w_down, post_gain):
     own_normed = rms_scale(tokens.astype(jnp.float32), norm_gain).astype(jnp.bfloat16)
-    normed = lax.all_gather(own_normed, "tp", axis=0, tiled=True)
+    normed = rest_pools(own_normed)
     gate = jnp.dot(
         normed, lax.all_gather(w_gate, "fs", axis=0, tiled=True), preferred_element_type=jnp.float32
     )

time: 276 us -> 251 us (0.909)
  waiting for transfers between devices: 242 us -> 212 us
  local copies, waits for them, and re-layouts: 0.01 us -> 5.03 us
    all_gather x1, waiting for transfers between devices: 63.5 us -> 30.7 us  [body(): lax.all_gather(w_up, 'fs', axis=0, tiled=True)]
    ppermute x0 -> x3, waiting for transfers between devices: none -> 26 us  [_place_rows(): then[s] = lax.ppermute(then[s + 1], along_axis, series)]
    all_gather x1 -> x0, waiting for transfers between devices: 23.3 us -> none  [body(): normed = lax.all_gather(own_normed, 'tp', axis=0, tiled=True)]
    all_gather x1, waiting for transfers between devices: 65 us -> 59.4 us  [body(): lax.all_gather(w_gate, 'fs', axis=0, tiled=True)]
    all_gather x1, waiting for transfers between devices: 58.2 us -> 63.7 us  [body(): lax.all_gather(w_down, 'fs', axis=1, tiled=True)]
    unnamed x4 -> x12, local copies, waits for them, and re-layouts: 0.01 us -> 5.03 us
  transfers between devices with their start and end apart: 5 -> 7, of which waited for: 5 -> 7; matrix products, arithmetic and copies ran while one was open for 2% -> 5% of each run, Pallas kernels for 0% -> 0%
where the time goes in v1:
time: 251 us
  waiting for transfers between devices  212 us (84%)
  between operations  13.2 us (5%)
  matrix products  13.1 us (5%)
  other arithmetic  7.33 us (3%)
  local copies, waits for them, and re-layouts  5.03 us (2%)
    all_gather x1, waiting for transfers between devices, body(): lax.all_gather(w_down, 'fs', axis=1, tiled=True)  63.7 us
    all_gather x1, waiting for transfers between devices, body(): lax.all_gather(w_gate, 'fs', axis=0, tiled=True)  59.4 us
    all_gather x1, waiting for transfers between devices, body(): lax.all_gather(w_up, 'fs', axis=0, tiled=True)  30.7 us
    reduce_scatter x1, waiting for transfers between devices, body(): lax.psum_scatter(terms.astype(jnp.bfloat16), 'tp', scatter_dimension=0, t...  30 us
    ppermute x3, waiting for transfers between devices, _place_rows(): then[s] = lax.ppermute(then[s + 1], along_axis, series)  26 us
    dot_general x1, matrix products, body(): jnp.dot(hidden, lax.all_gather(w_down, 'fs', axis=1, tiled=True), preferr...  8.82 us
    unnamed x12, local copies, waits for them, and re-layouts  5.03 us
  transfers between devices with their start and end apart: 7, of which 7 were waited for; matrix products, arithmetic and copies ran while one was open for 5% of the time, Pallas kernels for 0%

profile of v1, /device:TPU:0, one launch (start us, length us, event | category | flops | bytes accessed | tf_op | source)
XLA Modules:
  0.0 251.1 jit_solution(12599917524785784371)
XLA Ops:
  6.5 0.7 all-gather.6.cloned.1.call-update
  7.3 0.0 copy-start.1
  7.3 0.0 all-gather.4.cloned.1.call-start
  7.3 0.7 all-gather.4.cloned.1.call-update
  8.0 0.0 all-gather.8.cloned.1.call-start
  8.1 0.7 all-gather.8.cloned.1.call-update
  8.8 0.0 reduce-scatter.2.cloned.1.call-start
  8.8 1.2 fusion.4
  10.0 0.9 fusion.6
  10.9 0.5 collective-permute-start
  11.5 8.8 %collective-permute-done = bf16[128,2048]{1,0:T(8,128)(2,1)S(1)} collective-permute-done((bf16[128,2048]{1,0:T(8,128)(2,1)S(1)}, bf16[128,2048]{1,0:T(8,128)(2,1)S(1)}, u32[]{:S(2)}, u32[]{:S(2)}) %collective-permute-start) | collective-permute-done | bytes 524320 | tf_op jit(solution)/shard_map/ppermute | solution.py:16
  20.3 8.6 %collective-permute-done.1 = bf16[128,2048]{1,0:T(8,128)(2,1)S(1)} collective-permute-done((bf16[128,2048]{1,0:T(8,128)(2,1)S(1)}, bf16[128,2048]{1,0:T(8,128)(2,1)S(1)}, u32[]{:S(2)}, u32[]{:S(2)}) %collective-permute-start.1) | collective-permute-done | bytes 524320 | tf_op jit(solution)/shard_map/ppermute | solution.py:16
  28.9 0.0 collective-permute-start.2
  28.9 8.6 %collective-permute-done.2 = bf16[128,2048]{1,0:T(8,128)(2,1)S(1)} collective-permute-done((bf16[128,2048]{1,0:T(8,128)(2,1)S(1)}, bf16[128,2048]{1,0:T(8,128)(2,1)S(1)}, u32[]{:S(2)}, u32[]{:S(2)}) %collective-permute-start.2) | collective-permute-done | bytes 524320 | tf_op jit(solution)/shard_map/ppermute | solution.py:16
  37.5 0.8 constant_dynamic-update-slice_fusion.7
  38.3 0.8 constant_dynamic-update-slice_fusion.6
  39.1 0.9 constant_dynamic-update-slice_fusion.5
  40.0 1.0 constant_dynamic-update-slice_fusion.4
  41.0 0.8 constant_dynamic-update-slice_fusion.3
  41.8 0.8 constant_dynamic-update-slice_fusion.2
  42.6 0.8 constant_dynamic-update-slice_fusion.1
  43.5 1.0 constant_dynamic-update-slice_fusion
  44.4 30.7 %all-gather.6.cloned.1.call-done = bf16[2048,768]{1,0:T(8,128)(2,1)} async-done(((bf16[512,768]{1,0:T(8,128)(2,1)}), bf16[2048,768]{1,0:T(8,128)(2,1)}) %all-gather.6.cloned.1.call-update) | async-done | bytes 3145744 | tf_op jit(solution)/shard_map/all_gather | solution.py:36
  75.1 4.3 %fusion = f32[512,768]{1,0:T(8,128)S(1)} fusion(bf16[2048,768]{1,0:T(8,128)(2,1)} %all-gather.6.cloned.1.call-done, bf16[1024,2048]{1,0:T(8,128)(2,1)} %constant_dynamic-update-slice_fusion, s32[]{:T(128)S(6)} %select_n.14), kind=kOutput, calls=%fused_computation.1 | convolution fusion | flops 1610612736 | bytes 6815748 | tf_op jit(solution)/shard_map/dot_general | solution.py:35
  79.4 0.0 copy-start.2
  79.4 59.4 %all-gather.4.cloned.1.call-done = bf16[2048,768]{1,0:T(8,128)(2,1)} async-done(((bf16[512,768]{1,0:T(8,128)(2,1)}), bf16[2048,768]{1,0:T(8,128)(2,1)}) %all-gather.4.cloned.1.call-update) | async-done | bytes 3145744 | tf_op jit(solution)/shard_map/all_gather | solution.py:33
  138.8 63.7 %all-gather.8.cloned.1.call-done = bf16[768,2048]{1,0:T(8,128)(2,1)} async-done(((bf16[768,512]{1,0:T(8,128)(2,1)}), bf16[768,2048]{1,0:T(8,128)(2,1)}) %all-gather.8.cloned.1.call-update) | async-done | bytes 3145744 | tf_op jit(solution)/shard_map/all_gather | solution.py:40
  202.5 8.8 %convolution_convert_fusion = bf16[512,2048]{1,0:T(8,128)(2,1)} fusion(bf16[768,2048]{1,0:T(8,128)(2,1)} %all-gather.8.cloned.1.call-done, f32[512,768]{1,0:T(8,128)S(1)} %fusion, bf16[2048,768]{1,0:T(8,128)(2,1)} %all-gather.4.cloned.1.call-done, bf16[1024,2048]{1,0:T(8,128)(2,1)} %constant_dynamic-update-slice_fusion, s32[]{:T(128)S(6)} %select_n.14), kind=kOutput, calls=%fused_computation | convolution fusion | flops 3224633344 | bytes 12058628 | tf_op jit(solution)/shard_map/dot_general | solution.py:39
  211.3 0.0 reduce-scatter.2.cloned.1.call-update
  211.3 30.0 %reduce-scatter.2.cloned.1.call-done = bf16[128,2048]{1,0:T(8,128)(2,1)} async-done(((bf16[512,2048]{1,0:T(8,128)(2,1)}), bf16[128,2048]{1,0:T(8,128)(2,1)}) %reduce-scatter.2.cloned.1.call-update) | async-done | bytes 524304 | tf_op jit(solution)/shard_map/reduce_scatter | solution.py:42
  241.3 1.2 fusion.7
  242.6 2.0 fusion.9
  (8 shorter events, 0.0 us)
Async XLA Ops:
  6.5 3.5 %copy-start = (bf16[128,2048]{1,0:T(8,128)(2,1)S(1)}, bf16[128,2048]{1,0:T(8,128)(2,1)}, u32[]{:S(2)}) copy-start(bf16[128,2048]{1,0:T(8,128)(2,1)} %param.6) | copy-start | bytes 1572868
  6.5 68.6 %all-gather.6.cloned.1.call-start = ((), (), s32[]{:S(2)}) async-start(), calls=%async_computation.2 | async-start | bytes 3932160 | tf_op jit(solution)/shard_map/all_gather | solution.py:36
  7.3 32.7 %copy-start.1 = (f32[2048]{0:T(1024)S(1)}, f32[2048]{0:T(1024)}, u32[]{:S(2)}) copy-start(f32[2048]{0:T(1024)} %param.7) | copy-start | bytes 24580
  7.3 131.5 %all-gather.4.cloned.1.call-start = ((), (), s32[]{:S(2)}) async-start(), calls=%async_computation.1 | async-start | bytes 3932160 | tf_op jit(solution)/shard_map/all_gather | solution.py:33
  8.0 194.5 %all-gather.8.cloned.1.call-start = ((), (), s32[]{:S(2)}) async-start(), calls=%async_computation.3 | async-start | bytes 3932160 | tf_op jit(solution)/shard_map/all_gather | solution.py:40
  8.8 232.6 %reduce-scatter.2.cloned.1.call-start = ((), (), s32[]{:S(2)}) async-start(), calls=%async_computation.4 | async-start | bytes 2621440 | tf_op jit(solution)/shard_map/reduce_scatter | solution.py:42
  10.9 9.3 %collective-permute-start = (bf16[128,2048]{1,0:T(8,128)(2,1)S(1)}, bf16[128,2048]{1,0:T(8,128)(2,1)S(1)}, u32[]{:S(2)}, u32[]{:S(2)}) collective-permute-start(bf16[128,2048]{1,0:T(8,128)(2,1)S(1)} %fusion.6), channel_id=1, source_target_pairs={{0,1},{1,2},{2,3},{3,0},{4,5},{5,6},{6,7},{7,4},{8,9},{9,10},{10,1... | collective-permute-start | bytes 1572872 | tf_op jit(solution)/shard_map/ppermute | solution.py:16
  20.3 8.6 %collective-permute-start.1 = (bf16[128,2048]{1,0:T(8,128)(2,1)S(1)}, bf16[128,2048]{1,0:T(8,128)(2,1)S(1)}, u32[]{:S(2)}, u32[]{:S(2)}) collective-permute-start(bf16[128,2048]{1,0:T(8,128)(2,1)S(1)} %collective-permute-done), channel_id=1, source_target_pairs={{0,1},{1,2},{2,3},{3,0},{4,5},{5,6},{6,7},{7,4},{8,9},{9,10},{10,1... | collective-permute-start | bytes 1572872 | tf_op jit(solution)/shard_map/ppermute | solution.py:16
  28.9 8.6 %collective-permute-start.2 = (bf16[128,2048]{1,0:T(8,128)(2,1)S(1)}, bf16[128,2048]{1,0:T(8,128)(2,1)S(1)}, u32[]{:S(2)}, u32[]{:S(2)}) collective-permute-start(bf16[128,2048]{1,0:T(8,128)(2,1)S(1)} %collective-permute-done.1), channel_id=1, source_target_pairs={{0,1},{1,2},{2,3},{3,0},{4,5},{5,6},{6,7},{7,4},{8,9},{9,10},{10,1... | collective-permute-start | bytes 1572872 | tf_op jit(solution)/shard_map/ppermute | solution.py:16
  79.4 163.1 %copy-start.2 = (f32[2048]{0:T(1024)S(1)}, f32[2048]{0:T(1024)}, u32[]{:S(2)}) copy-start(f32[2048]{0:T(1024)} %param.11) | copy-start | bytes 24580
Sparse Core Ops, SparseCore 0:
  8.9 66.1 all-gather.5
  76.7 62.0 all-gather.3
  140.4 62.0 all-gather.7
  211.4 29.8 reduce-scatter.1
